TPU v7x, 256 devices: a 2x2x32 block of a 4x16x32 slice. The times are simulated.
256 devices in a mesh: grp: 4 (over y, x), ep: 32 (over z), tp: 2 (over core).
Axes of the slice: x: 2, y: 2, z: 32, core: 2. Of those that a mesh axis runs over, the one named last changes fastest.
The devices are a block of a 4x16x32 slice.
Arguments:
- tokens: bfloat16 [32768, 2048], P(('grp', 'ep')), parts along dimension 0, may hold values from -6 to 6
- picks: int32 [32, 4096], P(None, ('grp', 'ep')), parts along dimension 1, may hold values from 0 to 8191, as said below
- route_weights: bfloat16 [32, 4096], P(None, ('grp', 'ep')), parts along dimension 1, may hold values from 0.19921875 to 1
- gate_weight: bfloat16 [32, 2048, 1024], P('ep', None, 'tp'), may hold values from -0.125 to 0.125
- up_weight: bfloat16 [32, 2048, 1024], P('ep', None, 'tp'), may hold values from -0.125 to 0.125
- down_weight: bfloat16 [32, 1024, 2048], P('ep', 'tp'), may hold values from -0.1875 to 0.1875
Outputs:
- mixed: bfloat16 [32768, 2048], P(('grp', 'ep'), 'tp'), parts along dimension 0
There are 4 independent parts, one for each index of `grp`. A program takes and returns all parts, laid end to end along the dimension named above; an argument that names none is the same for every part. Nothing has to cross between parts.
Inputs may be any that keep to these rules, and one draw needn't show every extreme that they name: `picks`: slots k * 32 to (k + 1) * 32 - 1 of every expert name 32 different tokens of the block k * 256 to (k + 1) * 256 - 1.
All inputs are finite; a program needn't handle non-finite values.
Results may differ from a plain program's by a relative error of at most 0.0066.
Values may be sent and summed in bfloat16 or wider, within the bound.
A program may use at most 64 MiB of HBM per device.

v0:
```python
import math

import jax
import jax.numpy as jnp
from jax import lax
from jax.sharding import PartitionSpec as P

TOK_DEV = 256


def side_by_side(arrays, axis, split_dim, concat_dim, along):
    widths = [math.prod(a.shape[along:]) for a in arrays]
    both = jnp.concatenate(
        [a.reshape(*a.shape[:along], w) for a, w in zip(arrays, widths)], axis=along
    )
    result = lax.all_to_all(both, axis, split_axis=split_dim, concat_axis=concat_dim, tiled=True)
    tiles = jnp.split(result, [sum(widths[:k]) for k in range(1, len(widths))], axis=along)
    return tuple(
        (b.reshape(*result.shape[:along], *a.shape[along:]) for a, b in zip(arrays, tiles))
    )


def side_by_side_2(arrays, axis, dim, along):
    widths = [math.prod(a.shape[along:]) for a in arrays]
    both = jnp.concatenate(
        [a.reshape(*a.shape[:along], w) for a, w in zip(arrays, widths)], axis=along
    )
    result = lax.all_gather(both, axis, axis=dim, tiled=True)
    tiles = jnp.split(result, [sum(widths[:k]) for k in range(1, len(widths))], axis=along)
    return tuple(
        (b.reshape(*result.shape[:along], *a.shape[along:]) for a, b in zip(arrays, tiles))
    )


def split_up(shard, dim, size):
    dims = shard.shape
    tiles = shard.reshape(*dims[:dim], size, dims[dim] // size, *dims[dim + 1 :])
    return jnp.moveaxis(tiles, dim, 0)


def summed_on_arrival(shard, axis, dim):
    size = lax.axis_size(axis)
    tiles = lax.all_to_all(split_up(shard, dim, size), axis, 0, 0, tiled=True)
    return jnp.sum(tiles.astype(jnp.float32), axis=0)


def cut_rows(length, count):
    turn = length // count
    if turn >= 8:
        turn -= turn % 8
    return [turn * k for k in range(1, count)]


def in_order(tiles, dim):
    tiles = jnp.moveaxis(tiles, 0, dim)
    dims = tiles.shape
    return tiles.reshape(*dims[:dim], dims[dim] * dims[dim + 1], *dims[dim + 2 :])


def several_exchanges(shard, axis, pieces, split_dim, concat_dim):
    tiles = split_up(shard, split_dim, lax.axis_size(axis))
    widest = max(range(1, max(2, tiles.ndim - 1)), key=lambda d: tiles.shape[d])
    outs = []
    for section in jnp.split(tiles, cut_rows(tiles.shape[widest], pieces), axis=widest):
        if section.size:
            outs.append(lax.all_to_all(section, axis, split_axis=0, concat_axis=0, tiled=True))
    return in_order(jnp.concatenate(outs, axis=widest), concat_dim)


def per_device(tokens, picks, route_weights, gate_weight, up_weight, down_weight):
    experts, per = picks.shape
    width = tokens.shape[1]
    owners = lax.axis_size("ep")
    exp_dev = experts // owners
    local_ids = picks % TOK_DEV
    half = per // 2
    offset = lax.axis_index("tp") * half
    ids_half = lax.dynamic_slice_in_dim(local_ids, offset, half, 1)
    weights_half = lax.dynamic_slice_in_dim(route_weights, offset, half, 1)
    rows = jnp.take(tokens, ids_half, axis=0)
    got_rows, got_weights = side_by_side((rows, weights_half), "ep", 0, 1, 2)
    got_rows = got_rows.reshape(exp_dev, owners, half, width)
    got_weights = got_weights.reshape(exp_dev, owners, half)
    got_rows, got_weights = side_by_side_2((got_rows, got_weights), "tp", 2, 3)
    got_rows = got_rows.reshape(exp_dev, owners * per, width)
    got_weights = got_weights.reshape(exp_dev, owners * per)
    gate = jnp.einsum("ecd,edf->ecf", got_rows, gate_weight, preferred_element_type=jnp.float32)
    up = jnp.einsum("ecd,edf->ecf", got_rows, up_weight, preferred_element_type=jnp.float32)
    hidden = (jax.nn.silu(gate) * up * got_weights.astype(jnp.float32)[:, :, None]).astype(
        jnp.bfloat16
    )
    partial_value = jnp.einsum(
        "ecf,efd->ecd", hidden, down_weight, preferred_element_type=jnp.float32
    ).astype(jnp.bfloat16)
    summed = summed_on_arrival(partial_value, "tp", 2)
    result = summed.astype(jnp.bfloat16)
    returned = several_exchanges(result, "ep", 2, 1, 0)
    flat = returned.reshape(experts * per, returned.shape[2])
    positions = lax.broadcasted_iota(jnp.int32, (TOK_DEV, experts * per), 0)
    onehot = (positions == local_ids.reshape(1, experts * per)).astype(jnp.bfloat16)
    mixed = jnp.dot(onehot, flat, preferred_element_type=jnp.float32)
    return mixed.astype(jnp.bfloat16)


def solution(mesh):
    return jax.shard_map(
        per_device,
        mesh=mesh,
        in_specs=(
            P(("grp", "ep"), None),
            P(None, ("grp", "ep")),
            P(None, ("grp", "ep")),
            P("ep", None, "tp"),
            P("ep", None, "tp"),
            P("ep", "tp", None),
        ),
        out_specs=P(("grp", "ep"), "tp"),
        check_vma=False,
    )
```

profile of v0, /device:TPU:37, one launch (start us, length us, event | category | flops | bytes accessed | tf_op | source)
XLA Modules:
  0.0 573.1 jit_solution(12907272286457111649)
XLA Ops:
  6.5 0.0 copy-start
  6.6 0.0 all-gather.2.cloned.1.call-start
  6.6 0.9 constant_dynamic-slice_fusion
  7.5 0.1 copy.18
  7.6 0.7 add_select_fusion
  8.3 0.1 compare_and_fusion
  8.4 0.1 reshape.74
  8.5 0.2 copy.15
  8.7 6.6 %gather_fusion = bf16[512,2048]{1,0:T(8,128)(2,1)} fusion(bf16[256,2048]{1,0:T(8,128)(2,1)} %param.6, s32[1024]{0:T(1024)S(1)} %pad_clamp_fusion), kind=kCustom, calls=%fused_computation | custom fusion | bytes 4196352 | tf_op jit(solution)/shard_map/jit(_take)/gather | solution.py:80
  15.3 1.8 broadcast_select_fusion
  17.2 0.2 pad_maximum_fusion
  17.3 243.0 %all_to_all.27 = bf16[32,16,2049]{2,1,0:T(8,128)(2,1)S(1)} all-to-all(bf16[32,16,2049]{2,1,0:T(8,128)(2,1)S(1)} %pad_maximum_fusion), channel_id=1, replica_groups=mesh['grp'=4,'ep'=32,'tp'=2] {'ep'}, dimensions={0} | all-to-all | bytes 4196352 | tf_op jit(solution)/shard_map/all_to_all | solution.py:16
  260.4 0.3 split.24
  260.7 1.6 pad_maximum_fusion.1
  262.3 0.1 all-gather.2.cloned.1.call-update
  262.3 15.2 %all-gather.2.cloned.1.call-done = bf16[1,32,32,2049]{3,2,1,0:T(8,128)(2,1)} async-done(((bf16[1,32,16,2049]{3,2,1,0:T(8,128)(2,1)}), bf16[1,32,32,2049]{3,2,1,0:T(8,128)(2,1)}) %all-gather.2.cloned.1.call-update) | async-done | bytes 4196368 | tf_op jit(solution)/shard_map/all_gather | solution.py:28
  277.5 1.2 convert_reduce_fusion
  278.7 0.1 reshape.71
  278.8 0.0 copy-start.2
  278.8 2.6 split.26
  281.4 0.0 copy-start.1
  281.4 2.0 copy-done.1
  283.4 0.0 copy-done.2
  283.4 3.7 fusion.1
  287.1 0.0 copy-done
  287.1 10.1 %convolution_convert_fusion = bf16[1024,2048]{1,0:T(8,128)(2,1)} fusion(bf16[1,512,2048]{2,1,0:T(8,128)(2,1)S(1)} %copy-done, f32[1024,512]{1,0:T(8,128)} %fusion.1, bf16[1024,2048]{1,0:T(8,128)(2,1)} %bitcast.34, bf16[1,2048,512]{2,1,0:T(8,128)(2,1)} %param.9, f32[1024]{0:T(1024)S(1)} %reshape.71), kind=kOutput, calls=%fused_computation.2 | convolution fusion | flops 4300734464 | bytes 14684160 | tf_op jit(solution)/shard_map/ecf,efd->ecd/dot_general | solution.py:92
  297.2 7.9 %reshape.70 = bf16[1,1024,2,1024]{3,2,1,0:T(2,128)(2,1)} reshape(bf16[1024,2048]{1,0:T(8,128)(2,1)} %convolution_convert_fusion) | data formatting | bytes 8388608 | tf_op jit(solution)/shard_map/reshape | solution.py:37
  305.0 3.5 copy.20
  308.5 8.1 %all_to_all.28 = bf16[2,1,1024,1024]{3,2,1,0:T(8,128)(2,1)} all-to-all(bf16[2,1,1024,1024]{3,2,1,0:T(8,128)(2,1)S(1)} %bitcast.27), channel_id=1, replica_groups=mesh['grp'=4,'ep'=32,'tp'=2] {'tp'}, dimensions={0} | all-to-all | bytes 8388608 | tf_op jit(solution)/shard_map/all_to_all | solution.py:43
  316.6 5.2 reduce_sum.12
  321.8 2.7 fusion.12
  324.5 126.2 %all_to_all.29 = bf16[32,1,16,1024]{3,2,1,0:T(8,128)(2,1)S(1)} all-to-all(bf16[32,1,16,1024]{3,2,1,0:T(8,128)(2,1)S(1)} %get-tuple-element.7), channel_id=1, replica_groups=mesh['grp'=4,'ep'=32,'tp'=2] {'ep'}, dimensions={0} | all-to-all | bytes 2097152 | tf_op jit(solution)/shard_map/all_to_all | solution.py:66
  450.7 8.0 %all-to-all-start.3 = ((bf16[32,1,16,1024]{3,2,1,0:T(8,128)(2,1)}), bf16[32,1,16,1024]{3,2,1,0:T(8,128)(2,1)}, u32[]{:S(2)}, u32[]{:S(2)}) async-start(bf16[32,1,16,1024]{3,2,1,0:T(8,128)(2,1)} %get-tuple-element.8), calls=%async_computation.3 | async-start | bytes 2097152 | tf_op jit(solution)/shard_map/all_to_all | solution.py:66
  458.7 0.1 eq.12
  458.8 104.5 %all-to-all-done.3 = bf16[32,1,16,1024]{3,2,1,0:T(8,128)(2,1)} async-done(((bf16[32,1,16,1024]{3,2,1,0:T(8,128)(2,1)}), bf16[32,1,16,1024]{3,2,1,0:T(8,128)(2,1)}, u32[]{:S(2)}, u32[]{:S(2)}) %all-to-all-start.3) | async-done | bytes 1048608 | tf_op jit(solution)/shard_map/all_to_all | solution.py:66
  563.3 1.4 pad_maximum_fusion.2
  564.7 1.5 convolution_convert_fusion.1
  (2 shorter events, 0.0 us)
Async XLA Ops:
  6.5 280.5 %copy-start = (bf16[1,512,2048]{2,1,0:T(8,128)(2,1)S(1)}, bf16[1,512,2048]{2,1,0:T(8,128)(2,1)}, u32[]{:S(2)}) copy-start(bf16[1,512,2048]{2,1,0:T(8,128)(2,1)} %param.11) | copy-start | bytes 6291460
  6.6 271.0 %all-gather.2.cloned.1.call-start = ((), (), s32[]{:S(2)}) async-start(), calls=%async_computation.4 | async-start | bytes 6684672 | tf_op jit(solution)/shard_map/all_gather | solution.py:28
  278.8 4.6 copy-start.2
  281.4 2.0 copy-start.1
  450.7 112.6 %all-to-all-start.3 = ((bf16[32,1,16,1024]{3,2,1,0:T(8,128)(2,1)}), bf16[32,1,16,1024]{3,2,1,0:T(8,128)(2,1)}, u32[]{:S(2)}, u32[]{:S(2)}) async-start(bf16[32,1,16,1024]{3,2,1,0:T(8,128)(2,1)} %get-tuple-element.8), calls=%async_computation.3 | async-start | bytes 2097152 | tf_op jit(solution)/shard_map/all_to_all | solution.py:66
Sparse Core Ops, SparseCore 0:
  262.4 15.0 all-gather.1
where the time goes:
time: 574 us; the launch traced here: 573 us
  blocking collectives  377 us (66%)
  waiting for transfers between devices  120 us (21%)
  local copies, waits for them, and re-layouts  27 us (5%)
  matrix products  15.3 us (3%)
  between operations  13.5 us (2%)
  other arithmetic  12.2 us (2%)
  starting transfers between devices  8.04 us (1%)
    all_to_all x1, blocking collectives, side_by_side(): lax.all_to_all(both, axis, split_axis=split_dim, concat_axis=concat_dim,...  243 us
    all_to_all x1, blocking collectives, several_exchanges(): lax.all_to_all(section, axis, split_axis=0, concat_axis=0, tiled=True)  126 us
    all_to_all x1, waiting for transfers between devices, several_exchanges(): lax.all_to_all(section, axis, split_axis=0, concat_axis=0, tiled=True)  104 us
    all_gather x1, waiting for transfers between devices, side_by_side_2(): result = lax.all_gather(both, axis, axis=dim, tiled=True)  15.2 us
  transfers between devices with their start and end apart: 2, of which 2 were waited for; matrix products, arithmetic and copies ran while one was open for 0% of the time, Pallas kernels for 0%

commit v1 on v0

v1 whole, which is shorter than its diff:
```python
import functools

import jax
import jax.numpy as jnp
from jax import lax
from jax.experimental import pallas as pl
from jax.experimental.pallas import tpu as pltpu
from jax.sharding import PartitionSpec as P

F32 = jnp.float32
BF16 = jnp.bfloat16
LANES = 128
HALF_LANES = 64


def dot(a, b):
    return lax.dot_general(a, b, (((1,), (0,)), ((), ())), preferred_element_type=F32)


def dot_nt(a, b):
    return lax.dot_general(a, b, (((1,), (1,)), ((), ())), preferred_element_type=F32)


def iota(shape, dim):
    return lax.broadcasted_iota(jnp.int32, shape, dim)


def fiota(shape, dim):
    return iota(shape, dim).astype(F32)


def ones_where(cond):
    return jnp.where(cond, 1.0, 0.0)


def kernel_body(
    n, tok_dev, per, dh, ff,
    tok_hbm, picks_ref, rw_ref, wg_hbm, wu_hbm, wd_hbm, out_ref,
    tok, wg, wu, wd, buf_l, buf_s, met_l, met_s, acc_l, acc_s, x, res, pin, pout, pw_l, pw_s, pw_own,
    back_l, back_s, load_sem, sd_l, rd_l, sd_s, rd_s, sm, rm, sx, rx, sp, rp, sc_l, rc_l, sc_s, rc_s,
):
    hops = n // 2
    dense = tok_dev // per
    big = 2 * per
    z = lax.axis_index("ep")
    t = lax.axis_index("tp")
    sign = 1 - 2 * t
    ahead = (lax.rem(z + sign + n, n), lax.rem(z - sign + n, n))
    behind = (ahead[1], ahead[0])
    buf, met, acc = (buf_l, buf_s), (met_l, met_s), (acc_l, acc_s)
    pw, back = (pw_l, pw_s), (back_l, back_s)
    sd, rd, sc, rc = (sd_l, sd_s), (rd_l, rd_s), (sc_l, sc_s), (rc_l, rc_s)

    def remote(src, dst, s, r, where):
        return pltpu.make_async_remote_copy(
            src_ref=src, dst_ref=dst, send_sem=s, recv_sem=r,
            device_id=where, device_id_type=pl.DeviceIdType.MESH,
        )

    def chunks(m):
        return (big, tok_dev // big) if m > dense else (per, m)

    def rows_of(m):
        return min(tok_dev, per * m)

    def span(c, rows):
        return pl.ds(c * rows, rows)

    def token_copy(d, k, c, rows):
        at = span(c, rows)
        return remote(
            buf[d].at[k, at], buf[d].at[k + 1, at], sd[d].at[k, c], rd[d].at[k + 1, c], {"ep": ahead[d]}
        )

    def token_arrival(d, k, c, rows):
        at = span(c, rows)
        return remote(buf[d].at[k, at], buf[d].at[k, at], sd[d].at[k, c], rd[d].at[k, c], {"ep": ahead[d]})

    def meta_copy(d, k):
        return remote(met[d].at[k], met[d].at[k + 1], sm.at[d, k], rm.at[d, k + 1], {"ep": ahead[d]})

    def meta_arrival(d, k):
        return remote(met[d].at[k], met[d].at[k], sm.at[d, k], rm.at[d, k], {"ep": ahead[d]})

    def sum_copy(d, k, c, rows):
        at = span(c, rows)
        return remote(
            acc[d].at[k, at], acc[d].at[k - 1, at], sc[d].at[k, c], rc[d].at[k - 1, c], {"ep": behind[d]}
        )

    def sum_arrival(d, k, c, rows):
        at = span(c, rows)
        return remote(acc[d].at[k, at], acc[d].at[k, at], sc[d].at[k, c], rc[d].at[k, c], {"ep": behind[d]})

    def slot_rows(slot):
        return pl.ds(slot * per, per)

    def row_copy(slot, part):
        at = x.at[part, slot_rows(slot)]
        return remote(at, at, sx.at[slot], rx.at[slot], {"tp": 1 - t})

    def part_copy(i, r0, rows):
        at = pl.ds(r0, rows)
        return remote(pout.at[at], pin.at[at], sp.at[i], rp.at[i], {"tp": 1 - t})

    def slot_of(d, k):
        return 2 * k - 1 + t if d == 0 else 2 * k - t

    barrier = pltpu.get_barrier_semaphore()
    for where in ({"ep": ahead[0]}, {"ep": ahead[1]}, {"tp": 1 - t}):
        pl.semaphore_signal(barrier, inc=1, device_id=where, device_id_type=pl.DeviceIdType.MESH)
    my_half = pl.ds(pl.multiple_of(t * dh, dh), dh)
    its_half = pl.ds(pl.multiple_of((1 - t) * dh, dh), dh)
    loads = [
        pltpu.make_async_copy(tok_hbm.at[:, my_half], tok, load_sem.at[0]),
        pltpu.make_async_copy(wg_hbm.at[0], wg, load_sem.at[1]),
        pltpu.make_async_copy(wu_hbm.at[0], wu, load_sem.at[2]),
        pltpu.make_async_copy(wd_hbm.at[0], wd, load_sem.at[3]),
    ]
    for copy in loads:
        copy.start()

    ids = (picks_ref[...] - z * tok_dev).astype(F32).astype(BF16)
    eye = ones_where(iota((per, per), 0) == iota((per, per), 1)).astype(BF16)
    ids_t = dot_nt(eye, ids)
    spread = ones_where(iota((n, LANES), 1) == iota((n, LANES), 0) + n).astype(BF16)
    weights_t = dot(dot_nt(eye, rw_ref[...]).astype(BF16), spread)
    lane_e = iota((per, n), 1)
    lane_t = fiota((per, tok_dev), 1)
    meta_lane = iota((per, LANES), 1)

    def chosen_by(e):
        column = jnp.sum(jnp.where(lane_e == e, ids_t, 0.0), axis=1, keepdims=True)
        return column == lane_t

    def reach(e, far):
        member = jnp.max(ones_where(chosen_by(e)), axis=0, keepdims=True)
        d_long = lax.rem((e - z) * sign + n, n)
        d_short = lax.rem(n - d_long, n)
        d_long = jnp.where(d_long <= hops, d_long, 0).astype(F32)
        d_short = jnp.where(d_short < hops, d_short, 0).astype(F32)
        return jnp.maximum(far[0], member * d_long), jnp.maximum(far[1], member * d_short)

    zero_row = jnp.zeros((1, tok_dev), F32)
    far = lax.fori_loop(0, n, reach, (zero_row, zero_row))
    eye_t = ones_where(iota((tok_dev, tok_dev), 0) == iota((tok_dev, tok_dev), 1)).astype(BF16)
    sub_t = fiota((tok_dev, tok_dev), 0)
    lane_tt = fiota((tok_dev, tok_dev), 1)
    orders = []
    for d in (0, 1):
        wide = jnp.broadcast_to(far[d], (LANES, tok_dev)).astype(BF16)
        column = dot_nt(eye_t, wide)[:, :1]
        key_row = far[d] * tok_dev - fiota((1, tok_dev), 1)
        key_col = column * tok_dev - fiota((tok_dev, 1), 0)
        place_row = jnp.sum(ones_where(key_col > key_row), axis=0, keepdims=True)
        place_col = jnp.sum(ones_where(key_row > key_col), axis=1, keepdims=True)
        orders.append(place_row)
        back[d][...] = ones_where(place_col == lane_tt).astype(BF16)

    def place_ids(e, tiles):
        picked = chosen_by(e)
        out = []
        for d in (0, 1):
            column = jnp.sum(jnp.where(picked, orders[d], 0.0), axis=1, keepdims=True)
            out.append(tiles[d] + jnp.where(meta_lane == e, column, 0.0))
        return tuple(out)

    tiles = lax.fori_loop(0, n, place_ids, (weights_t, weights_t))
    low = iota((per // 2, LANES), 1) < HALF_LANES
    for d in (0, 1):
        folded = jnp.where(low, tiles[d][: per // 2], pltpu.roll(tiles[d][per // 2 :], HALF_LANES, axis=1))
        met[d][0] = folded.astype(BF16)
    loads[0].wait()
    for d in (0, 1):
        swap = ones_where(orders[d] == sub_t).astype(BF16)
        buf[d][0] = dot(swap, tok[...]).astype(BF16)

    pl.semaphore_wait(barrier, 3)
    for d in (0, 1):
        meta_copy(d, 0).start()
    for c in range(tok_dev // big):
        for d in (0, 1):
            token_copy(d, 0, c, big).start()

    def pick_rows(id_col, weight_col, block, slot, store_back, rows):
        gather = ones_where(id_col == fiota((per, rows), 1)).astype(BF16)
        x[t, slot_rows(slot), :] = dot(gather, block).astype(BF16)
        row_copy(slot, t).start()
        square = iota((per, per), 0) == iota((per, per), 1)
        id_row = jnp.sum(jnp.where(square, id_col, 0.0), axis=0, keepdims=True)
        weight_row = jnp.sum(jnp.where(square, weight_col, 0.0), axis=0, keepdims=True)
        store_back(jnp.where(fiota((rows, per), 0) == id_row, weight_row, 0.0).astype(BF16))

    def own_rows():
        id_col = jnp.sum(jnp.where(lane_e == z, ids_t, 0.0), axis=1, keepdims=True)
        weight_col = jnp.sum(jnp.where(meta_lane == z + n, weights_t, 0.0), axis=1, keepdims=True)

        def store(value):
            pw_own[...] = value

        pick_rows(id_col, weight_col, tok[...], 0, store, tok_dev)

    def arrived_rows(d, k, rows):
        tile = met[d][k].astype(F32)
        lane = iota((per // 2, LANES), 1)

        def column(at):
            parts = [
                jnp.sum(jnp.where(lane == at + part, tile, 0.0), axis=1, keepdims=True)
                for part in (0, HALF_LANES)
            ]
            return jnp.concatenate(parts, axis=0)

        def store(value):
            pw[d][k, :rows] = value

        slot = slot_of(d, k)
        if not isinstance(k, int):
            pass
        elif k == hops:
            slot = n - 1
        pick_rows(column(z), column(z + n), buf[d][k, :rows], slot, store, rows)

    def token_step(q, m, both):
        pairs = ((0, q), (1, q - 1)) if both else ((0, q),)
        for d, k in pairs:
            meta_arrival(d, k).wait_recv()
            if m > 1:
                meta_copy(d, k).start()
        rows_in, n_in = chunks(m)
        rows_out, n_out = chunks(m - 1)
        each = rows_in // rows_out
        for c in range(n_in):
            for d, k in pairs:
                token_arrival(d, k, c, rows_in).wait_recv()
                for piece in range(c * each, (c + 1) * each):
                    if piece < n_out:
                        token_copy(d, k, piece, rows_out).start()
        for d, k in pairs:
            arrived_rows(d, k, rows_of(m))

    fc = min(ff, 256)
    dc = min(dh, 512)

    def feed_forward(i, first, last):
        r0, rows = first * per, (last - first) * per

        @pl.loop(first, last)
        def _(slot):
            row_copy(slot, 1 - t).wait_recv()

        at = pl.ds(r0, rows)
        hidden = []
        for f in range(0, ff, fc):
            cols = pl.ds(f, fc)
            gate = dot(x[0, at, :], wg[:dh, cols]) + dot(x[1, at, :], wg[dh:, cols])
            up = dot(x[0, at, :], wu[:dh, cols]) + dot(x[1, at, :], wu[dh:, cols])
            hidden.append((gate / (1.0 + jnp.exp(-gate)) * up).astype(BF16))
        hidden = jnp.concatenate(hidden, axis=1)
        pout[at, :] = dot(hidden, wd[:, its_half]).astype(BF16)
        part_copy(i, r0, rows).start()
        mine = dot(hidden, wd[:, my_half]).astype(BF16).astype(F32)
        part_copy(i, r0, rows).wait_recv()
        res[at, :] = (mine + pin[at, :].astype(F32)).astype(BF16)

    own_rows()
    for copy in loads[1:]:
        copy.wait()
    token_step(1, hops, False)
    last_uniform = hops - dense - 1
    quarter = n // 4
    bounds = [0, quarter + 1, 2 * quarter + 1, 3 * quarter + 1, n]

    def uniform_steps(first, last):
        if last >= first:

            @pl.loop(first, last + 1)
            def _(q):
                token_step(q, hops, True)

    ready = [(bounds[i + 1] - 1) // 2 + 2 for i in range(3)]
    q = 2
    for i in range(4):
        until = hops if i == 3 else ready[i]
        stop = min(until, last_uniform)
        uniform_steps(q, stop)
        q = max(q, stop + 1)
        while q <= until:
            token_step(q, hops + 1 - q, True)
            q += 1
        feed_forward(i, bounds[i], bounds[i + 1])

    def add_to(d, k, slot, at):
        return dot(pw[d][k, at], res[slot_rows(slot), :])

    def sum_step(q, m, both):
        pairs = ((0, q), (1, q - 1)) if both else ((0, q),)
        rows_out, n_out = chunks(m)
        rows_in, n_in = chunks(m - 1)
        each = rows_out // rows_in
        order = [n_out - 1] + list(range(n_out - 1)) if m <= dense else list(range(n_out))
        for c in order:
            for d, k in pairs:
                slot = slot_of(d, k)
                if isinstance(k, int) and k == hops:
                    slot = n - 1
                at = span(c, rows_out)
                value = add_to(d, k, slot, at)
                if c * each < n_in:
                    for piece in range(c * each, (c + 1) * each):
                        sum_arrival(d, k, piece, rows_in).wait_recv()
                    value = value + acc[d][k, at].astype(F32)
                acc[d][k, at] = value.astype(BF16)
                sum_copy(d, k, c, rows_out).start()

    q = hops
    while q > 1:
        m = hops + 1 - q
        if m > dense + 1:

            @pl.loop(0, q - 1)
            def _(i):
                sum_step(q - i, m, True)

            break
        sum_step(q, m, True)
        q -= 1
    sum_step(1, hops, False)

    for d in (0, 1):
        for k in range(hops - d):
            m = hops - k - d
            rows, count = chunks(m)
            for c in range(count):
                token_copy(d, k, c, rows).wait_send()
                sum_copy(d, k + 1, c, rows).wait_send()
            meta_copy(d, k).wait_send()

    @pl.loop(0, n)
    def _(slot):
        row_copy(slot, t).wait_send()

    for i in range(4):
        part_copy(i, bounds[i] * per, (bounds[i + 1] - bounds[i]) * per).wait_send()

    total = dot(pw_own[...], res[slot_rows(0), :])
    for d in (1, 0):
        for c in range(tok_dev // big):
            sum_arrival(d, 0, c, big).wait_recv()
        total = total + dot(back[d][...], acc[d][0])
    out_ref[...] = total.astype(BF16)


def per_device(tokens, picks, route_weights, gate_weight, up_weight, down_weight):
    n = lax.axis_size("ep")
    tok_dev, width = tokens.shape
    per = picks.shape[1]
    ff = down_weight.shape[1]
    dh = width // lax.axis_size("tp")
    hops = n // 2
    most = tok_dev // per
    dma = pltpu.SemaphoreType.DMA
    vmem = pltpu.VMEM
    kernel = pl.pallas_call(
        functools.partial(kernel_body, n, tok_dev, per, dh, ff),
        out_shape=jax.ShapeDtypeStruct((tok_dev, dh), BF16),
        in_specs=[
            pl.BlockSpec(memory_space=pl.ANY),
            pl.BlockSpec(memory_space=vmem),
            pl.BlockSpec(memory_space=vmem),
            pl.BlockSpec(memory_space=pl.ANY),
            pl.BlockSpec(memory_space=pl.ANY),
            pl.BlockSpec(memory_space=pl.ANY),
        ],
        out_specs=pl.BlockSpec(memory_space=vmem),
        scratch_shapes=[
            vmem((tok_dev, dh), BF16),
            vmem((width, ff), BF16),
            vmem((width, ff), BF16),
            vmem((ff, width), BF16),
            vmem((hops + 1, tok_dev, dh), BF16),
            vmem((hops, tok_dev, dh), BF16),
            vmem((hops + 1, per // 2, LANES), BF16),
            vmem((hops, per // 2, LANES), BF16),
            vmem((hops + 1, tok_dev, dh), BF16),
            vmem((hops, tok_dev, dh), BF16),
            vmem((2, n * per, dh), BF16),
            vmem((n * per, dh), BF16),
            vmem((n * per, dh), BF16),
            vmem((n * per, dh), BF16),
            vmem((hops + 1, tok_dev, per), BF16),
            vmem((hops, tok_dev, per), BF16),
            vmem((tok_dev, per), BF16),
            vmem((tok_dev, tok_dev), BF16),
            vmem((tok_dev, tok_dev), BF16),
            dma((4,)),
            dma((hops + 1, most)), dma((hops + 1, most)), dma((hops, most)), dma((hops, most)),
            dma((2, hops + 1)), dma((2, hops + 1)),
            dma((n,)), dma((n,)),
            dma((4,)), dma((4,)),
            dma((hops + 1, most)), dma((hops + 1, most)), dma((hops, most)), dma((hops, most)),
        ],
        compiler_params=pltpu.CompilerParams(
            collective_id=0, has_side_effects=True, vmem_limit_bytes=67043328
        ),
    )
    return kernel(tokens, picks, route_weights, gate_weight, up_weight, down_weight)


def solution(mesh):
    return jax.shard_map(
        per_device,
        mesh=mesh,
        in_specs=(
            P(("grp", "ep"), None),
            P(None, ("grp", "ep")),
            P(None, ("grp", "ep")),
            P("ep", None, "tp"),
            P("ep", None, "tp"),
            P("ep", "tp", None),
        ),
        out_specs=P(("grp", "ep"), "tp"),
        check_vma=False,
    )
```

time: 574 us -> 331 us (0.58)
  blocking collectives: 377 us -> 0 us
  Pallas kernels: 0 us -> 329 us
  waiting for transfers between devices: 120 us -> 0 us
  local copies, waits for them, and re-layouts: 27 us -> 1.87 us
  matrix products: 15.3 us -> 0 us
  between operations: 13.5 us -> 0.01 us
  other arithmetic: 12.2 us -> 0 us
  starting transfers between devices: 8.04 us -> 0 us
    all_to_all x3 -> x0, blocking collectives: 377 us -> none  [the longest x1 243 us: side_by_side(): lax.all_to_all(both, axis, split_axis=split_dim, concat_axis=concat_dim,...]
    pallas_call x0 -> x1, Pallas kernels: none -> 329 us  [per_device(): kernel(tokens, picks, route_weights, gate_weight, up_weight, down_weight)]
    all_to_all x1 -> x0, waiting for transfers between devices: 104 us -> none  [several_exchanges(): lax.all_to_all(section, axis, split_axis=0, concat_axis=0, tiled=True)]
    dot_general x3 -> x0, matrix products: 15.3 us -> none  [the longest x1 10.1 us: per_device(): jnp.einsum('ecf,efd->ecd', hidden, down_weight, preferred_element_type=jn...]
    all_gather x1 -> x0, waiting for transfers between devices: 15.2 us -> none  [side_by_side_2(): result = lax.all_gather(both, axis, axis=dim, tiled=True)]
    reshape x3 -> x0, local copies, waits for them, and re-layouts: 11.5 us -> none  [the longest x2 11.3 us: split_up(): tiles = shard.reshape(*dims[:dim], size, dims[dim] // size, *dims[dim + 1:])]
    all_to_all x1 -> x0, starting transfers between devices: 8.03 us -> none  [several_exchanges(): lax.all_to_all(section, axis, split_axis=0, concat_axis=0, tiled=True)]
    gather x1 -> x0, local copies, waits for them, and re-layouts: 6.63 us -> none  [per_device(): rows = jnp.take(tokens, ids_half, axis=0)]
  transfers between devices with their start and end apart: 2 -> 0, of which waited for: 2 -> 0; matrix products, arithmetic and copies ran while one was open for 0% -> 0% of each run, Pallas kernels for 0% -> 0%
where the time goes in v1:
time: 331 us
  Pallas kernels  329 us (99%)
    pallas_call x1, Pallas kernels, per_device(): kernel(tokens, picks, route_weights, gate_weight, up_weight, down_weight)  329 us

profile of v1, /device:TPU:37, one launch (start us, length us, event | category | flops | bytes accessed | tf_op | source)
XLA Modules:
  0.0 331.3 jit_solution(11172448676575117808)
XLA Ops:
  0.0 329.4 %shard_map.64 = bf16[256,1024]{1,0:T(8,128)(2,1)} custom-call(bf16[256,2048]{1,0:T(8,128)(2,1)} %tok_hbm.1, s32[32,32]{1,0:T(8,128)} %picks_ref.1, bf16[32,32]{1,0:T(8,128)(2,1)} %rw_ref.1, bf16[1,2048,512]{2,1,0:T(8,128)(2,1)} %wg_hbm.1, bf16[1,2048,512]{2,1,0:T(8,128)(2,1)} %wu_hbm.1, bf16[1,512,2048]{2,1,0:T(8,128)(2,1)} %wd_hbm.1), custom_call_target="tpu_custom_call" | custom-call | tf_op jit(solution)/shard_map/pallas_call | solution.py:407
  329.4 1.9 copy.8

commit v2 on v1

--- a/solution.py
+++ b/solution.py
@@ -36,7 +36,7 @@
 def kernel_body(
     n, tok_dev, per, dh, ff,
     tok_hbm, picks_ref, rw_ref, wg_hbm, wu_hbm, wd_hbm, out_ref,
-    tok, wg, wu, wd, buf_l, buf_s, met_l, met_s, acc_l, acc_s, x, res, pin, pout, pw_l, pw_s, pw_own,
+    tok, wg, wu, wd, buf_l, buf_s, met_l, met_s, acc_l, acc_s, x, res, pin, pout, pw_l, pw_s, pw_own, scale,
     back_l, back_s, load_sem, sd_l, rd_l, sd_s, rd_s, sm, rm, sx, rx, sp, rp, sc_l, rc_l, sc_s, rc_s,
 ):
     hops = n // 2
@@ -63,17 +63,20 @@
     def rows_of(m):
         return min(tok_dev, per * m)
 
+    def pieces(m, part):
+        return range(part * (dense // 2), min(m, (part + 1) * (dense // 2)))
+
     def span(c, rows):
         return pl.ds(c * rows, rows)
 
-    def token_copy(d, k, c, rows):
-        at = span(c, rows)
+    def token_copy(d, k, c):
+        at = span(c, per)
         return remote(
             buf[d].at[k, at], buf[d].at[k + 1, at], sd[d].at[k, c], rd[d].at[k + 1, c], {"ep": ahead[d]}
         )
 
-    def token_arrival(d, k, c, rows):
-        at = span(c, rows)
+    def token_arrival(d, k, c):
+        at = span(c, per)
         return remote(buf[d].at[k, at], buf[d].at[k, at], sd[d].at[k, c], rd[d].at[k, c], {"ep": ahead[d]})
 
     def meta_copy(d, k):
@@ -142,10 +145,19 @@
         return jnp.maximum(far[0], member * d_long), jnp.maximum(far[1], member * d_short)
 
     zero_row = jnp.zeros((1, tok_dev), F32)
-    far = lax.fori_loop(0, n, reach, (zero_row, zero_row))
+    trip = min(n, 8)
+
+    def several(step):
+        def run(i, carry):
+            for j in range(trip):
+                carry = step(i * trip + j, carry)
+            return carry
+
+        return run
+
+    far = lax.fori_loop(0, n // trip, several(reach), (zero_row, zero_row))
     eye_t = ones_where(iota((tok_dev, tok_dev), 0) == iota((tok_dev, tok_dev), 1)).astype(BF16)
     sub_t = fiota((tok_dev, tok_dev), 0)
-    lane_tt = fiota((tok_dev, tok_dev), 1)
     orders = []
     for d in (0, 1):
         wide = jnp.broadcast_to(far[d], (LANES, tok_dev)).astype(BF16)
@@ -155,7 +167,8 @@
         place_row = jnp.sum(ones_where(key_col > key_row), axis=0, keepdims=True)
         place_col = jnp.sum(ones_where(key_row > key_col), axis=1, keepdims=True)
         orders.append(place_row)
-        back[d][...] = ones_where(place_col == lane_tt).astype(BF16)
+        for c in range(tok_dev // big):
+            back[d][c] = ones_where(place_col == fiota((tok_dev, big), 1) + c * big).astype(BF16)
 
     def place_ids(e, tiles):
         picked = chosen_by(e)
@@ -165,7 +178,7 @@
             out.append(tiles[d] + jnp.where(meta_lane == e, column, 0.0))
         return tuple(out)
 
-    tiles = lax.fori_loop(0, n, place_ids, (weights_t, weights_t))
+    tiles = lax.fori_loop(0, n // trip, several(place_ids), (weights_t, weights_t))
     low = iota((per // 2, LANES), 1) < HALF_LANES
     for d in (0, 1):
         folded = jnp.where(low, tiles[d][: per // 2], pltpu.roll(tiles[d][per // 2 :], HALF_LANES, axis=1))
@@ -178,18 +191,22 @@
     pl.semaphore_wait(barrier, 3)
     for d in (0, 1):
         meta_copy(d, 0).start()
-    for c in range(tok_dev // big):
-        for d in (0, 1):
-            token_copy(d, 0, c, big).start()
+
+    def own_block(part):
+        for c in pieces(hops, part):
+            for d in (0, 1):
+                token_copy(d, 0, c).start()
+
+    own_block(0)
 
     def pick_rows(id_col, weight_col, block, slot, store_back, rows):
+        scale[slot_rows(slot), :] = weight_col
         gather = ones_where(id_col == fiota((per, rows), 1)).astype(BF16)
         x[t, slot_rows(slot), :] = dot(gather, block).astype(BF16)
         row_copy(slot, t).start()
         square = iota((per, per), 0) == iota((per, per), 1)
         id_row = jnp.sum(jnp.where(square, id_col, 0.0), axis=0, keepdims=True)
-        weight_row = jnp.sum(jnp.where(square, weight_col, 0.0), axis=0, keepdims=True)
-        store_back(jnp.where(fiota((rows, per), 0) == id_row, weight_row, 0.0).astype(BF16))
+        store_back(ones_where(fiota((rows, per), 0) == id_row).astype(BF16))
 
     def own_rows():
         id_col = jnp.sum(jnp.where(lane_e == z, ids_t, 0.0), axis=1, keepdims=True)
@@ -221,26 +238,24 @@
             slot = n - 1
         pick_rows(column(z), column(z + n), buf[d][k, :rows], slot, store, rows)
 
-    def token_step(q, m, both):
+    def token_step(part, q, m, both=True):
         pairs = ((0, q), (1, q - 1)) if both else ((0, q),)
-        for d, k in pairs:
-            meta_arrival(d, k).wait_recv()
-            if m > 1:
-                meta_copy(d, k).start()
-        rows_in, n_in = chunks(m)
-        rows_out, n_out = chunks(m - 1)
-        each = rows_in // rows_out
-        for c in range(n_in):
+        if part == 0:
             for d, k in pairs:
-                token_arrival(d, k, c, rows_in).wait_recv()
-                for piece in range(c * each, (c + 1) * each):
-                    if piece < n_out:
-                        token_copy(d, k, piece, rows_out).start()
-        for d, k in pairs:
-            arrived_rows(d, k, rows_of(m))
+                meta_arrival(d, k).wait_recv()
+                if m > 1:
+                    meta_copy(d, k).start()
+        onward = pieces(m - 1, part)
+        for c in pieces(m, part):
+            for d, k in pairs:
+                token_arrival(d, k, c).wait_recv()
+                if c in onward:
+                    token_copy(d, k, c).start()
+        if part == (0 if m <= dense // 2 else 1):
+            for d, k in pairs:
+                arrived_rows(d, k, rows_of(m))
 
     fc = min(ff, 256)
-    dc = min(dh, 512)
 
     def feed_forward(i, first, last):
         r0, rows = first * per, (last - first) * per
@@ -255,40 +270,13 @@
             cols = pl.ds(f, fc)
             gate = dot(x[0, at, :], wg[:dh, cols]) + dot(x[1, at, :], wg[dh:, cols])
             up = dot(x[0, at, :], wu[:dh, cols]) + dot(x[1, at, :], wu[dh:, cols])
-            hidden.append((gate / (1.0 + jnp.exp(-gate)) * up).astype(BF16))
+            hidden.append((gate / (1.0 + jnp.exp(-gate)) * up * scale[at, :]).astype(BF16))
         hidden = jnp.concatenate(hidden, axis=1)
         pout[at, :] = dot(hidden, wd[:, its_half]).astype(BF16)
         part_copy(i, r0, rows).start()
         mine = dot(hidden, wd[:, my_half]).astype(BF16).astype(F32)
         part_copy(i, r0, rows).wait_recv()
         res[at, :] = (mine + pin[at, :].astype(F32)).astype(BF16)
-
-    own_rows()
-    for copy in loads[1:]:
-        copy.wait()
-    token_step(1, hops, False)
-    last_uniform = hops - dense - 1
-    quarter = n // 4
-    bounds = [0, quarter + 1, 2 * quarter + 1, 3 * quarter + 1, n]
-
-    def uniform_steps(first, last):
-        if last >= first:
-
-            @pl.loop(first, last + 1)
-            def _(q):
-                token_step(q, hops, True)
-
-    ready = [(bounds[i + 1] - 1) // 2 + 2 for i in range(3)]
-    q = 2
-    for i in range(4):
-        until = hops if i == 3 else ready[i]
-        stop = min(until, last_uniform)
-        uniform_steps(q, stop)
-        q = max(q, stop + 1)
-        while q <= until:
-            token_step(q, hops + 1 - q, True)
-            q += 1
-        feed_forward(i, bounds[i], bounds[i + 1])
 
     def add_to(d, k, slot, at):
         return dot(pw[d][k, at], res[slot_rows(slot), :])
@@ -313,26 +301,68 @@
                 acc[d][k, at] = value.astype(BF16)
                 sum_copy(d, k, c, rows_out).start()
 
-    q = hops
-    while q > 1:
-        m = hops + 1 - q
-        if m > dense + 1:
-
-            @pl.loop(0, q - 1)
-            def _(i):
-                sum_step(q - i, m, True)
-
-            break
-        sum_step(q, m, True)
-        q -= 1
+    def experts_left(q):
+        return hops + 1 - q
+
+    bounds = [0, hops // 2 - 1, hops - 1, 3 * hops // 2 + 1, n]
+
+    def some_experts(i):
+        feed_forward(i, bounds[i], bounds[i + 1])
+
+    def tokens_of(part, q):
+        token_step(part, q, experts_left(q))
+
+    def sums_of(q):
+        sum_step(q, experts_left(q), True)
+
+    own_rows()
+    for copy in loads[1:]:
+        copy.wait()
+    full = hops - dense // 2
+    token_step(0, 1, hops, False)
+
+    @pl.loop(2, full + 1)
+    def _(q):
+        token_step(0, q, hops, True)
+
+    own_block(1)
+    for i in range(dense // 2):
+        tokens_of(0, full + 1 + i)
+        token_step(1, 1 + i, experts_left(1 + i), i > 0)
+    some_experts(3)
+    tokens_of(1, dense // 2 + 1)
+    some_experts(0)
+
+    @pl.loop(dense // 2 + 2, hops - dense + 1)
+    def _(q):
+        token_step(1, q, hops, True)
+
+    tokens_of(1, hops - dense + 1)
+    some_experts(1)
+    back_hop = hops
+    for q in range(hops - dense + 2, full + 1):
+        sums_of(back_hop)
+        back_hop -= 1
+        tokens_of(1, q)
+    some_experts(2)
+    while experts_left(back_hop) <= dense + 1:
+        sums_of(back_hop)
+        back_hop -= 1
+    rest = back_hop
+
+    @pl.loop(0, rest - 1)
+    def _(i):
+        sum_step(rest - i, hops, True)
+
     sum_step(1, hops, False)
 
     for d in (0, 1):
         for k in range(hops - d):
             m = hops - k - d
             rows, count = chunks(m)
+            for c in range(min(m, dense)):
+                token_copy(d, k, c).wait_send()
             for c in range(count):
-                token_copy(d, k, c, rows).wait_send()
                 sum_copy(d, k + 1, c, rows).wait_send()
             meta_copy(d, k).wait_send()
 
@@ -347,7 +377,7 @@
     for d in (1, 0):
         for c in range(tok_dev // big):
             sum_arrival(d, 0, c, big).wait_recv()
-        total = total + dot(back[d][...], acc[d][0])
+            total = total + dot(back[d][c], acc[d][0, span(c, big)])
     out_ref[...] = total.astype(BF16)
 
 
@@ -391,8 +421,9 @@
             vmem((hops + 1, tok_dev, per), BF16),
             vmem((hops, tok_dev, per), BF16),
             vmem((tok_dev, per), BF16),
-            vmem((tok_dev, tok_dev), BF16),
-            vmem((tok_dev, tok_dev), BF16),
+            vmem((n * per, 1), F32),
+            vmem((tok_dev // (2 * per), tok_dev, 2 * per), BF16),
+            vmem((tok_dev // (2 * per), tok_dev, 2 * per), BF16),
             dma((4,)),
             dma((hops + 1, most)), dma((hops + 1, most)), dma((hops, most)), dma((hops, most)),
             dma((2, hops + 1)), dma((2, hops + 1)),

time: 331 us -> 323 us (0.976)
  Pallas kernels: 329 us -> 321 us
    pallas_call x1, Pallas kernels: 329 us -> 321 us  [per_device(): kernel(tokens, picks, route_weights, gate_weight, up_weight, down_weight)]
where the time goes in v2:
time: 323 us
  Pallas kernels  321 us (99%)
    pallas_call x1, Pallas kernels, per_device(): kernel(tokens, picks, route_weights, gate_weight, up_weight, down_weight)  321 us

profile of v2, /device:TPU:37, one launch (start us, length us, event | category | flops | bytes accessed | tf_op | source)
XLA Modules:
  0.0 323.1 jit_solution(10278375424006571286)
XLA Ops:
  0.0 321.2 %shard_map.64 = bf16[256,1024]{1,0:T(8,128)(2,1)} custom-call(bf16[256,2048]{1,0:T(8,128)(2,1)} %tok_hbm.1, s32[32,32]{1,0:T(8,128)} %picks_ref.1, bf16[32,32]{1,0:T(8,128)(2,1)} %rw_ref.1, bf16[1,2048,512]{2,1,0:T(8,128)(2,1)} %wg_hbm.1, bf16[1,2048,512]{2,1,0:T(8,128)(2,1)} %wu_hbm.1, bf16[1,512,2048]{2,1,0:T(8,128)(2,1)} %wd_hbm.1), custom_call_target="tpu_custom_call" | custom-call | tf_op jit(solution)/shard_map/pallas_call | solution.py:438
  321.2 1.9 copy.8

commit v3 on v2

--- a/solution.py
+++ b/solution.py
@@ -158,17 +158,32 @@
     far = lax.fori_loop(0, n // trip, several(reach), (zero_row, zero_row))
     eye_t = ones_where(iota((tok_dev, tok_dev), 0) == iota((tok_dev, tok_dev), 1)).astype(BF16)
     sub_t = fiota((tok_dev, tok_dev), 0)
-    orders = []
+    keys, orders, swaps = [], [], []
     for d in (0, 1):
         wide = jnp.broadcast_to(far[d], (LANES, tok_dev)).astype(BF16)
         column = dot_nt(eye_t, wide)[:, :1]
         key_row = far[d] * tok_dev - fiota((1, tok_dev), 1)
         key_col = column * tok_dev - fiota((tok_dev, 1), 0)
         place_row = jnp.sum(ones_where(key_col > key_row), axis=0, keepdims=True)
-        place_col = jnp.sum(ones_where(key_row > key_col), axis=1, keepdims=True)
+        keys.append((key_row, key_col))
         orders.append(place_row)
-        for c in range(tok_dev // big):
-            back[d][c] = ones_where(place_col == fiota((tok_dev, big), 1) + c * big).astype(BF16)
+        swaps.append(ones_where(place_row == sub_t).astype(BF16))
+
+    def own_block(part):
+        rows = tok_dev // 2
+        for d in (0, 1):
+            at = slice(part * rows, (part + 1) * rows)
+            buf[d][0, at] = dot(swaps[d][at], tok[...]).astype(BF16)
+
+    def send_own_block(part):
+        for c in pieces(hops, part):
+            for d in (0, 1):
+                token_copy(d, 0, c).start()
+
+    loads[0].wait()
+    own_block(0)
+    pl.semaphore_wait(barrier, 3)
+    send_own_block(0)
 
     def place_ids(e, tiles):
         picked = chosen_by(e)
@@ -183,21 +198,13 @@
     for d in (0, 1):
         folded = jnp.where(low, tiles[d][: per // 2], pltpu.roll(tiles[d][per // 2 :], HALF_LANES, axis=1))
         met[d][0] = folded.astype(BF16)
-    loads[0].wait()
-    for d in (0, 1):
-        swap = ones_where(orders[d] == sub_t).astype(BF16)
-        buf[d][0] = dot(swap, tok[...]).astype(BF16)
-
-    pl.semaphore_wait(barrier, 3)
+    own_block(1)
     for d in (0, 1):
         meta_copy(d, 0).start()
-
-    def own_block(part):
-        for c in pieces(hops, part):
-            for d in (0, 1):
-                token_copy(d, 0, c).start()
-
-    own_block(0)
+        key_row, key_col = keys[d]
+        place_col = jnp.sum(ones_where(key_row > key_col), axis=1, keepdims=True)
+        for c in range(tok_dev // big):
+            back[d][c] = ones_where(place_col == fiota((tok_dev, big), 1) + c * big).astype(BF16)
 
     def pick_rows(id_col, weight_col, block, slot, store_back, rows):
         scale[slot_rows(slot), :] = weight_col
@@ -240,17 +247,17 @@
 
     def token_step(part, q, m, both=True):
         pairs = ((0, q), (1, q - 1)) if both else ((0, q),)
-        if part == 0:
-            for d, k in pairs:
-                meta_arrival(d, k).wait_recv()
-                if m > 1:
-                    meta_copy(d, k).start()
         onward = pieces(m - 1, part)
         for c in pieces(m, part):
             for d, k in pairs:
                 token_arrival(d, k, c).wait_recv()
                 if c in onward:
                     token_copy(d, k, c).start()
+        if part == 0:
+            for d, k in pairs:
+                meta_arrival(d, k).wait_recv()
+                if m > 1:
+                    meta_copy(d, k).start()
         if part == (0 if m <= dense // 2 else 1):
             for d, k in pairs:
                 arrived_rows(d, k, rows_of(m))
@@ -274,9 +281,13 @@
         hidden = jnp.concatenate(hidden, axis=1)
         pout[at, :] = dot(hidden, wd[:, its_half]).astype(BF16)
         part_copy(i, r0, rows).start()
-        mine = dot(hidden, wd[:, my_half]).astype(BF16).astype(F32)
+        res[at, :] = dot(hidden, wd[:, my_half]).astype(BF16)
+
+    def join_halves(i, first, last):
+        r0, rows = first * per, (last - first) * per
+        at = pl.ds(r0, rows)
         part_copy(i, r0, rows).wait_recv()
-        res[at, :] = (mine + pin[at, :].astype(F32)).astype(BF16)
+        res[at, :] = (res[at, :].astype(F32) + pin[at, :].astype(F32)).astype(BF16)
 
     def add_to(d, k, slot, at):
         return dot(pw[d][k, at], res[slot_rows(slot), :])
@@ -304,10 +315,13 @@
     def experts_left(q):
         return hops + 1 - q
 
-    bounds = [0, hops // 2 - 1, hops - 1, 3 * hops // 2 + 1, n]
+    bounds = [0, hops // 2 - 1, hops - 1, 5 * hops // 4 + 1, 3 * hops // 2 + 1, n]
 
     def some_experts(i):
         feed_forward(i, bounds[i], bounds[i + 1])
+
+    def join(i):
+        join_halves(i, bounds[i], bounds[i + 1])
 
     def tokens_of(part, q):
         token_step(part, q, experts_left(q))
@@ -325,18 +339,20 @@
     def _(q):
         token_step(0, q, hops, True)
 
-    own_block(1)
+    send_own_block(1)
     for i in range(dense // 2):
         tokens_of(0, full + 1 + i)
         token_step(1, 1 + i, experts_left(1 + i), i > 0)
-    some_experts(3)
+    some_experts(4)
     tokens_of(1, dense // 2 + 1)
+    join(4)
     some_experts(0)
 
     @pl.loop(dense // 2 + 2, hops - dense + 1)
     def _(q):
         token_step(1, q, hops, True)
 
+    join(0)
     tokens_of(1, hops - dense + 1)
     some_experts(1)
     back_hop = hops
@@ -344,7 +360,12 @@
         sums_of(back_hop)
         back_hop -= 1
         tokens_of(1, q)
-    some_experts(2)
+        if q == full - 1:
+            join(1)
+            some_experts(2)
+    some_experts(3)
+    join(2)
+    join(3)
     while experts_left(back_hop) <= dense + 1:
         sums_of(back_hop)
         back_hop -= 1
@@ -370,7 +391,7 @@
     def _(slot):
         row_copy(slot, t).wait_send()
 
-    for i in range(4):
+    for i in range(5):
         part_copy(i, bounds[i] * per, (bounds[i + 1] - bounds[i]) * per).wait_send()
 
     total = dot(pw_own[...], res[slot_rows(0), :])
@@ -428,7 +449,7 @@
             dma((hops + 1, most)), dma((hops + 1, most)), dma((hops, most)), dma((hops, most)),
             dma((2, hops + 1)), dma((2, hops + 1)),
             dma((n,)), dma((n,)),
-            dma((4,)), dma((4,)),
+            dma((5,)), dma((5,)),
             dma((hops + 1, most)), dma((hops + 1, most)), dma((hops, most)), dma((hops, most)),
         ],
         compiler_params=pltpu.CompilerParams(

time: 323 us -> 317 us (0.981)
  Pallas kernels: 321 us -> 315 us
    pallas_call x1, Pallas kernels: 321 us -> 315 us  [per_device(): kernel(tokens, picks, route_weights, gate_weight, up_weight, down_weight)]
where the time goes in v3:
time: 317 us; the launch traced here: 316 us
  Pallas kernels  315 us (99%)
    pallas_call x1, Pallas kernels, per_device(): kernel(tokens, picks, route_weights, gate_weight, up_weight, down_weight)  315 us

profile of v3, /device:TPU:37, one launch (start us, length us, event | category | flops | bytes accessed | tf_op | source)
XLA Modules:
  0.0 316.5 jit_solution(4510038674678102423)
XLA Ops:
  0.0 314.6 %shard_map.64 = bf16[256,1024]{1,0:T(8,128)(2,1)} custom-call(bf16[256,2048]{1,0:T(8,128)(2,1)} %tok_hbm.1, s32[32,32]{1,0:T(8,128)} %picks_ref.1, bf16[32,32]{1,0:T(8,128)(2,1)} %rw_ref.1, bf16[1,2048,512]{2,1,0:T(8,128)(2,1)} %wg_hbm.1, bf16[1,2048,512]{2,1,0:T(8,128)(2,1)} %wu_hbm.1, bf16[1,512,2048]{2,1,0:T(8,128)(2,1)} %wd_hbm.1), custom_call_target="tpu_custom_call" | custom-call | tf_op jit(solution)/shard_map/pallas_call | solution.py:459
  314.6 1.9 copy.8

commit v4 on v3

--- a/solution.py
+++ b/solution.py
@@ -36,7 +36,7 @@
 def kernel_body(
     n, tok_dev, per, dh, ff,
     tok_hbm, picks_ref, rw_ref, wg_hbm, wu_hbm, wd_hbm, out_ref,
-    tok, wg, wu, wd, buf_l, buf_s, met_l, met_s, acc_l, acc_s, x, res, pin, pout, pw_l, pw_s, pw_own, scale,
+    tok, wg, wu, wd, buf_l, buf_s, met_l, met_s, acc_l, acc_s, x, res, pin, pout, pw_l, pw_s, pw_own, scale, hid,
     back_l, back_s, load_sem, sd_l, rd_l, sd_s, rd_s, sm, rm, sx, rx, sp, rp, sc_l, rc_l, sc_s, rc_s,
 ):
     hops = n // 2
@@ -245,43 +245,54 @@
             slot = n - 1
         pick_rows(column(z), column(z + n), buf[d][k, :rows], slot, store, rows)
 
-    def token_step(part, q, m, both=True):
+    def token_step(part, q, m, both=True, tasks=()):
         pairs = ((0, q), (1, q - 1)) if both else ((0, q),)
         onward = pieces(m - 1, part)
-        for c in pieces(m, part):
+        arriving = pieces(m, part)
+        for j, c in enumerate(arriving):
             for d, k in pairs:
                 token_arrival(d, k, c).wait_recv()
                 if c in onward:
                     token_copy(d, k, c).start()
+            for task in tasks[j * len(tasks) // len(arriving) : (j + 1) * len(tasks) // len(arriving)]:
+                task()
         if part == 0:
             for d, k in pairs:
                 meta_arrival(d, k).wait_recv()
                 if m > 1:
                     meta_copy(d, k).start()
-        if part == (0 if m <= dense // 2 else 1):
-            for d, k in pairs:
-                arrived_rows(d, k, rows_of(m))
+
+    def take_rows(q):
+        rows = rows_of(hops + 1 - q)
+        pairs = ((0, q), (1, q - 1)) if q > 1 else ((0, q),)
+        return [functools.partial(arrived_rows, d, k, rows) for d, k in pairs]
 
     fc = min(ff, 256)
 
     def feed_forward(i, first, last):
         r0, rows = first * per, (last - first) * per
-
-        @pl.loop(first, last)
-        def _(slot):
-            row_copy(slot, 1 - t).wait_recv()
-
         at = pl.ds(r0, rows)
-        hidden = []
-        for f in range(0, ff, fc):
+
+        def enter():
+            @pl.loop(first, last)
+            def _(slot):
+                row_copy(slot, 1 - t).wait_recv()
+
+        def units(f):
             cols = pl.ds(f, fc)
             gate = dot(x[0, at, :], wg[:dh, cols]) + dot(x[1, at, :], wg[dh:, cols])
             up = dot(x[0, at, :], wu[:dh, cols]) + dot(x[1, at, :], wu[dh:, cols])
-            hidden.append((gate / (1.0 + jnp.exp(-gate)) * up * scale[at, :]).astype(BF16))
-        hidden = jnp.concatenate(hidden, axis=1)
-        pout[at, :] = dot(hidden, wd[:, its_half]).astype(BF16)
-        part_copy(i, r0, rows).start()
-        res[at, :] = dot(hidden, wd[:, my_half]).astype(BF16)
+            hid[at, cols] = (gate / (1.0 + jnp.exp(-gate)) * up * scale[at, :]).astype(BF16)
+
+        def down_for_partner():
+            pout[at, :] = dot(hid[at, :], wd[:, its_half]).astype(BF16)
+            part_copy(i, r0, rows).start()
+
+        def down():
+            res[at, :] = dot(hid[at, :], wd[:, my_half]).astype(BF16)
+
+        blocks = [functools.partial(units, f) for f in range(0, ff, fc)]
+        return [enter] + blocks + [down_for_partner, down]
 
     def join_halves(i, first, last):
         r0, rows = first * per, (last - first) * per
@@ -315,16 +326,23 @@
     def experts_left(q):
         return hops + 1 - q
 
-    bounds = [0, hops // 2 - 1, hops - 1, 5 * hops // 4 + 1, 3 * hops // 2 + 1, n]
+    bounds = [0] + [2 * k - 1 for k in (hops // 4, 7 * hops // 16, 5 * hops // 8, 13 * hops // 16)] + [n]
 
     def some_experts(i):
-        feed_forward(i, bounds[i], bounds[i + 1])
+        return feed_forward(i, bounds[i], bounds[i + 1])
 
     def join(i):
         join_halves(i, bounds[i], bounds[i + 1])
 
-    def tokens_of(part, q):
-        token_step(part, q, experts_left(q))
+    def tokens_of(part, q, tasks=()):
+        token_step(part, q, experts_left(q), q > 1, tasks)
+
+    def run(tasks):
+        for task in tasks:
+            task()
+
+    def joined(i):
+        return functools.partial(join, i)
 
     def sums_of(q):
         sum_step(q, experts_left(q), True)
@@ -340,30 +358,28 @@
         token_step(0, q, hops, True)
 
     send_own_block(1)
-    for i in range(dense // 2):
-        tokens_of(0, full + 1 + i)
-        token_step(1, 1 + i, experts_left(1 + i), i > 0)
-    some_experts(4)
-    tokens_of(1, dense // 2 + 1)
-    join(4)
-    some_experts(0)
-
-    @pl.loop(dense // 2 + 2, hops - dense + 1)
-    def _(q):
-        token_step(1, q, hops, True)
-
-    join(0)
-    tokens_of(1, hops - dense + 1)
-    some_experts(1)
+    near = 0
+    for q in range(full + 1, hops + 1):
+        tokens_of(0, q)
+        tokens_of(1, near + 1, take_rows(q) + (take_rows(near) if near else []))
+        near += 1
+    far_tasks, near_tasks = some_experts(4), some_experts(0)
+    tokens_of(1, near + 1, take_rows(near) + far_tasks[:2])
+    tokens_of(1, near + 2, take_rows(near + 1) + far_tasks[2:])
+    tokens_of(1, near + 3, take_rows(near + 2) + [joined(4)] + near_tasks[:2])
+    tokens_of(1, near + 4, take_rows(near + 3) + near_tasks[2:])
+    tokens_of(1, near + 5, take_rows(near + 4) + some_experts(1) + [joined(0)])
+    run(take_rows(near + 5))
     back_hop = hops
-    for q in range(hops - dense + 2, full + 1):
+    for q in range(near + 6, full + 1):
         sums_of(back_hop)
         back_hop -= 1
         tokens_of(1, q)
-        if q == full - 1:
+        run(take_rows(q))
+        if q == full - 2:
             join(1)
-            some_experts(2)
-    some_experts(3)
+            run(some_experts(2))
+    run(some_experts(3))
     join(2)
     join(3)
     while experts_left(back_hop) <= dense + 1:
@@ -443,6 +459,7 @@
             vmem((hops, tok_dev, per), BF16),
             vmem((tok_dev, per), BF16),
             vmem((n * per, 1), F32),
+            vmem((n * per, ff), BF16),
             vmem((tok_dev // (2 * per), tok_dev, 2 * per), BF16),
             vmem((tok_dev // (2 * per), tok_dev, 2 * per), BF16),
             dma((4,)),

time: 317 us -> 319 us (level)
  no operation moved by 1% of the time
where the time goes in v4:
time: 319 us
  Pallas kernels  317 us (99%)
    pallas_call x1, Pallas kernels, per_device(): kernel(tokens, picks, route_weights, gate_weight, up_weight, down_weight)  317 us

profile of v4, /device:TPU:37, one launch (start us, length us, event | category | flops | bytes accessed | tf_op | source)
XLA Modules:
  0.0 318.7 jit_solution(2960196236007723369)
XLA Ops:
  0.0 316.8 %shard_map.64 = bf16[256,1024]{1,0:T(8,128)(2,1)} custom-call(bf16[256,2048]{1,0:T(8,128)(2,1)} %tok_hbm.1, s32[32,32]{1,0:T(8,128)} %picks_ref.1, bf16[32,32]{1,0:T(8,128)(2,1)} %rw_ref.1, bf16[1,2048,512]{2,1,0:T(8,128)(2,1)} %wg_hbm.1, bf16[1,2048,512]{2,1,0:T(8,128)(2,1)} %wu_hbm.1, bf16[1,512,2048]{2,1,0:T(8,128)(2,1)} %wd_hbm.1), custom_call_target="tpu_custom_call" | custom-call | tf_op jit(solution)/shard_map/pallas_call | solution.py:476
  316.8 1.9 copy.8

commit v5 on v3

--- a/solution.py
+++ b/solution.py
@@ -324,7 +324,7 @@
         join_halves(i, bounds[i], bounds[i + 1])
 
     def tokens_of(part, q):
-        token_step(part, q, experts_left(q))
+        token_step(part, q, experts_left(q), q > 1)
 
     def sums_of(q):
         sum_step(q, experts_left(q), True)
@@ -333,32 +333,34 @@
     for copy in loads[1:]:
         copy.wait()
     full = hops - dense // 2
+    alone = full - 2
     token_step(0, 1, hops, False)
 
-    @pl.loop(2, full + 1)
+    @pl.loop(2, alone + 1)
     def _(q):
         token_step(0, q, hops, True)
 
     send_own_block(1)
-    for i in range(dense // 2):
-        tokens_of(0, full + 1 + i)
-        token_step(1, 1 + i, experts_left(1 + i), i > 0)
+    near = 1
+    for q in range(alone + 1, hops + 1):
+        tokens_of(0, q)
+        tokens_of(1, near)
+        if near == hops // 4 + 1:
+            some_experts(0)
+        near += 1
     some_experts(4)
-    tokens_of(1, dense // 2 + 1)
+    tokens_of(1, near)
+    join(0)
     join(4)
-    some_experts(0)
-
-    @pl.loop(dense // 2 + 2, hops - dense + 1)
-    def _(q):
-        token_step(1, q, hops, True)
-
-    join(0)
+    for q in range(near + 1, hops - dense + 1):
+        tokens_of(1, q)
     tokens_of(1, hops - dense + 1)
-    some_experts(1)
     back_hop = hops
     for q in range(hops - dense + 2, full + 1):
         sums_of(back_hop)
         back_hop -= 1
+        if q == hops - dense + 2:
+            some_experts(1)
         tokens_of(1, q)
         if q == full - 1:
             join(1)

time: 317 us -> 316 us (level)
  no operation moved by 1% of the time
where the time goes in v5:
time: 316 us
  Pallas kernels  314 us (99%)
    pallas_call x1, Pallas kernels, per_device(): kernel(tokens, picks, route_weights, gate_weight, up_weight, down_weight)  314 us

profile of v5, /device:TPU:37, one launch (start us, length us, event | category | flops | bytes accessed | tf_op | source)
XLA Modules:
  0.0 315.9 jit_solution(14769188056862760979)
XLA Ops:
  0.0 314.0 %shard_map.64 = bf16[256,1024]{1,0:T(8,128)(2,1)} custom-call(bf16[256,2048]{1,0:T(8,128)(2,1)} %tok_hbm.1, s32[32,32]{1,0:T(8,128)} %picks_ref.1, bf16[32,32]{1,0:T(8,128)(2,1)} %rw_ref.1, bf16[1,2048,512]{2,1,0:T(8,128)(2,1)} %wg_hbm.1, bf16[1,2048,512]{2,1,0:T(8,128)(2,1)} %wu_hbm.1, bf16[1,512,2048]{2,1,0:T(8,128)(2,1)} %wd_hbm.1), custom_call_target="tpu_custom_call" | custom-call | tf_op jit(solution)/shard_map/pallas_call | solution.py:461
  314.0 1.9 copy.8

commit v6 on v5

--- a/solution.py
+++ b/solution.py
@@ -292,8 +292,8 @@
     def add_to(d, k, slot, at):
         return dot(pw[d][k, at], res[slot_rows(slot), :])
 
-    def sum_step(q, m, both):
-        pairs = ((0, q), (1, q - 1)) if both else ((0, q),)
+    def sum_step(q, m, directions=(0, 1)):
+        pairs = [(d, q - d) for d in directions]
         rows_out, n_out = chunks(m)
         rows_in, n_in = chunks(m - 1)
         each = rows_out // rows_in
@@ -327,7 +327,7 @@
         token_step(part, q, experts_left(q), q > 1)
 
     def sums_of(q):
-        sum_step(q, experts_left(q), True)
+        sum_step(q, experts_left(q))
 
     own_rows()
     for copy in loads[1:]:
@@ -366,8 +366,11 @@
             join(1)
             some_experts(2)
     some_experts(3)
+    sum_step(back_hop, experts_left(back_hop), (0,))
     join(2)
     join(3)
+    sum_step(back_hop, experts_left(back_hop), (1,))
+    back_hop -= 1
     while experts_left(back_hop) <= dense + 1:
         sums_of(back_hop)
         back_hop -= 1
@@ -375,9 +378,9 @@
 
     @pl.loop(0, rest - 1)
     def _(i):
-        sum_step(rest - i, hops, True)
-
-    sum_step(1, hops, False)
+        sum_step(rest - i, hops)
+
+    sum_step(1, hops, (0,))
 
     for d in (0, 1):
         for k in range(hops - d):

time: 316 us -> 316 us (level)
  no operation moved by 1% of the time
where the time goes in v6:
time: 316 us
  Pallas kernels  314 us (99%)
    pallas_call x1, Pallas kernels, per_device(): kernel(tokens, picks, route_weights, gate_weight, up_weight, down_weight)  314 us

profile of v6, /device:TPU:37, one launch (start us, length us, event | category | flops | bytes accessed | tf_op | source)
XLA Modules:
  0.0 316.2 jit_solution(1925068449493465902)
XLA Ops:
  0.0 314.3 %shard_map.64 = bf16[256,1024]{1,0:T(8,128)(2,1)} custom-call(bf16[256,2048]{1,0:T(8,128)(2,1)} %tok_hbm.1, s32[32,32]{1,0:T(8,128)} %picks_ref.1, bf16[32,32]{1,0:T(8,128)(2,1)} %rw_ref.1, bf16[1,2048,512]{2,1,0:T(8,128)(2,1)} %wg_hbm.1, bf16[1,2048,512]{2,1,0:T(8,128)(2,1)} %wu_hbm.1, bf16[1,512,2048]{2,1,0:T(8,128)(2,1)} %wd_hbm.1), custom_call_target="tpu_custom_call" | custom-call | tf_op jit(solution)/shard_map/pallas_call | solution.py:464
  314.3 1.9 copy.8
